TPU v7x, 32 devices: a whole 2x2x4 slice. The times are simulated.
32 devices in a mesh: ra: 4 (over z), cb: 4 (over y, x), dp: 2 (over core).
Axes of the slice: x: 2, y: 2, z: 4, core: 2. Of those that a mesh axis runs over, the one named last changes fastest.
Arguments:
- stream: bfloat16 [4, 64, 4096], P('dp', None, 'ra'), may hold values from -16 to 16
- norm_gain: bfloat16 [2, 4096], P(None, 'ra'), may hold values from 0.099609375 to 1.8984375
- gate_weight: bfloat16 [2, 4096, 12288], P(None, 'ra', 'cb'), may hold values from -0.09375 to 0.09375
- value_weight: bfloat16 [2, 4096, 12288], P(None, 'ra', 'cb'), may hold values from -0.09375 to 0.09375
- gate_taps: bfloat16 [2, 3, 12288], P(None, None, 'cb'), may hold values from -3 to 3
- value_taps: bfloat16 [2, 3, 12288], P(None, None, 'cb'), may hold values from -3 to 3
- gate_bias: bfloat16 [2, 12288], P(None, 'cb'), may hold values from -3 to 3
- value_bias: bfloat16 [2, 12288], P(None, 'cb'), may hold values from -3 to 3
- down_weight: bfloat16 [2, 12288, 4096], P(None, 'cb', 'ra'), may hold values from -0.0546875 to 0.0546875
- final_gain: bfloat16 [4096], P('ra'), may hold values from 0.099609375 to 1.8984375
Outputs:
- mixed: bfloat16 [4, 64, 4096], P('dp', None, 'ra')
All inputs are finite; a program needn't handle non-finite values.
Results may differ from a plain program's by a relative error of at most 0.035.
Values may be sent and summed in bfloat16 or wider, within the bound.
A program may use at most 128 MiB of HBM per device.

v0:
```python
import functools

import jax
import jax.numpy as jnp
from jax import lax
from jax.experimental import pallas as pl
from jax.experimental.pallas import tpu as pltpu
from jax.sharding import PartitionSpec as P

EPS = 1e-06
MESH = pl.DeviceIdType.MESH
LANES = 128
GROUPS = 2
CHUNKS = 6
SKEW = 2
SKEW_BACK = 2
LAG = 6
SKEW_CB = 2


def chain_kernel(
    dims,
    s_in, ng, gt, vt, gb, vb, fg, wg_hbm, wv_hbm, dn_hbm,
    out,
    wg, wv, dn, cur, u, part, rs_send, rs_recv, hid, acc, scale,
    sq_send, sq_recv, tbuf, rbuf, snew,
    wsem, wlate, dsem, rs_ss, rs_rs, ag_ss, ag_rs, sq_ss, sq_rs, t_ss, t_rs, n_ss, n_rs,
):
    n, m, width, length = dims
    layers, dl, ff = wg.shape
    groups, rows, _ = cur.shape
    chunks = part.shape[2]
    cw = ff // 2 // chunks
    rq = rows // m
    me = lax.axis_index("ra")
    mc = lax.axis_index("cb")
    head = SKEW * (n - 1)
    t_term = chunks + head + SKEW_BACK * (n - 1)
    t_own = t_term + SKEW_CB
    t_back = t_own + SKEW_CB
    per_layer = t_back + 1
    lag = LAG
    f32 = jnp.float32

    def wcopy(d, c, which):
        src, dst = ((wg_hbm, wg), (wv_hbm, wv))[which]
        cols = pl.ds(pl.multiple_of(d * (ff // 2) + c * cw, LANES), cw)
        return pltpu.make_async_copy(src.at[0, :, cols], dst.at[0, :, cols], wsem.at[which, d, c])

    def late(l, which):
        src, dst = ((wg_hbm, wg), (wv_hbm, wv))[which]
        return pltpu.make_async_copy(src.at[l], dst.at[l], wlate.at[which, l])

    def dcopy(l):
        return pltpu.make_async_copy(dn_hbm.at[l], dn.at[l], dsem.at[l])

    for c in range(chunks):
        for d in range(2):
            for which in range(2):
                wcopy(d, c, which).start()

    barrier = pltpu.get_barrier_semaphore()
    for o in range(1, n):
        pl.semaphore_signal(barrier, inc=1, device_id={"ra": lax.rem(me + o, n)}, device_id_type=MESH)
    for o in range(1, m):
        pl.semaphore_signal(barrier, inc=1, device_id={"cb": lax.rem(mc + o, m)}, device_id_type=MESH)
    pl.semaphore_wait(barrier, n + m - 2)

    def remote(src, dst, ss, rs, **to):
        return pltpu.make_async_remote_copy(
            src_ref=src, dst_ref=dst, send_sem=ss, recv_sem=rs, device_id=to, device_id_type=MESH
        )

    def toward(d, back):
        up = (d == 1) != back
        return lax.rem(me + (1 if up else n - 1), n)

    def rs_copy(l, h, d, c):
        return remote(
            rs_send.at[l, h, d, c], rs_recv.at[l, h, d, c], rs_ss.at[l, h, d, c], rs_rs.at[l, h, d, c],
            ra=toward(d, False),
        )

    def ag_copy(l, h, d, c):
        return remote(
            hid.at[l, h, d, c], hid.at[l, h, d, c], ag_ss.at[l, h, d, c], ag_rs.at[l, h, d, c],
            ra=toward(d, True),
        )

    def sq_copy(l, h, o):
        return remote(
            sq_send.at[l, h], sq_recv.at[l, h, o], sq_ss.at[l, h, o], sq_rs.at[l, h, o],
            ra=lax.rem(me + o, n),
        )

    def t_copy(l, h, o):
        to = lax.rem(mc + o, m)
        return remote(
            tbuf.at[l, h, pl.ds(pl.multiple_of(to * rq, rq), rq)], rbuf.at[l, h, o],
            t_ss.at[l, h, o], t_rs.at[l, h, o], cb=to,
        )

    def own(q):
        return pl.ds(pl.multiple_of(q * rq, rq), rq)

    def n_copy(l, h, o):
        mine = own(mc)
        return remote(
            snew.at[l, h, mine], snew.at[l, h, mine], n_ss.at[l, h, o], n_rs.at[l, h, o],
            cb=lax.rem(mc + o, m),
        )

    def n_wait(l, h, o):
        theirs = own(lax.rem(mc + m - o, m))
        remote(
            snew.at[l, h, theirs], snew.at[l, h, theirs], n_ss.at[l, h, o], n_rs.at[l, h, o],
            cb=lax.rem(mc + o, m),
        ).wait_recv()

    def row_of(ref, l, *at):
        block = ref[at].astype(f32)
        row = block[0:1]
        for i in range(1, layers):
            row = jnp.where(l == i, block[i : i + 1], row)
        return row

    def prep(h, l, s):
        cur[h] = s
        values = s.astype(f32)
        u[h] = (values * row_of(ng, l, slice(None), slice(None))).astype(jnp.bfloat16)
        total = jnp.sum(values * values, axis=1, keepdims=True)
        square = jnp.broadcast_to(jnp.concatenate([total] * (LANES // rows), axis=0), (LANES, LANES))
        sq_send[l, h] = square.T[0:8]
        for o in range(1, n):
            sq_copy(l, h, o).start()
        acc[h] = jnp.zeros((rows, dl), f32)

    def finish_scale(h, l):
        total = sq_send[l, h]
        for o in range(1, n):
            sq_copy(l, h, o).wait_recv()
            total = total + sq_recv[l, h, o]
        inverse = lax.rsqrt(total / width + EPS)
        scale[h] = jnp.broadcast_to(inverse[0:1], (LANES, LANES)).T[0:rows]

    def down(h, l, d, c):
        at = pl.ds(pl.multiple_of(d * (ff // 2) + c * cw, LANES), cw)
        acc[h] += jnp.dot(hid[l, h, d, c], dn[l, at, :], preferred_element_type=f32)

    def mix(x, taps, bias):
        position = lax.rem(lax.broadcasted_iota(jnp.int32, x.shape, 0), length)
        count = len(taps)
        result = bias + x * taps[count - 1]
        for back in range(1, count):
            moved = jnp.where(position >= back, pltpu.roll(x, back, 0), 0.0)
            result = result + moved * taps[count - 1 - back]
        return result

    def hidden(h, l, d, c):
        cols = pl.ds(pl.multiple_of(d * (ff // 2) + c * cw, LANES), cw)
        factor = jnp.concatenate([scale[h]] * (cw // LANES), axis=1)
        gate = (part[h, d, c, :, :cw] + rs_recv[l, h, d, c, :, :cw].astype(f32)) * factor
        value = (part[h, d, c, :, cw:] + rs_recv[l, h, d, c, :, cw:].astype(f32)) * factor
        gate = mix(gate, [row_of(gt, l, i, slice(None), cols) for i in range(gt.shape[0])], row_of(gb, l, slice(None), cols))
        value = mix(value, [row_of(vt, l, i, slice(None), cols) for i in range(vt.shape[0])], row_of(vb, l, slice(None), cols))
        hid[l, h, d, c] = (jax.nn.gelu(gate) * value).astype(jnp.bfloat16)

    def step(h, l, tau):
        @pl.when(tau < chunks)
        def _():
            for d in range(2):
                if h == 0:

                    @pl.when(l == 0)
                    def _():
                        wcopy(d, tau, 0).wait()
                        wcopy(d, tau, 1).wait()

                    if d == 0:

                        @pl.when((l > 0) & (tau == 0))
                        def _():
                            late(l, 0).wait()
                            late(l, 1).wait()

                cols = pl.ds(pl.multiple_of(d * (ff // 2) + tau * cw, LANES), cw)
                part[h, d, tau, :, :cw] = jnp.dot(u[h], wg[l, :, cols], preferred_element_type=f32)
                part[h, d, tau, :, cw:] = jnp.dot(u[h], wv[l, :, cols], preferred_element_type=f32)

        @pl.when(tau == head)
        def _():
            finish_scale(h, l)
            if h == 0:
                dcopy(l).wait()

        for d in range(2):
            k = me if d == 1 else n - 1 - me
            c = tau - SKEW * k

            @pl.when((c >= 0) & (c < chunks))
            def _():
                @pl.when(k == 0)
                def _():
                    rs_send[l, h, d, c] = part[h, d, c].astype(jnp.bfloat16)
                    rs_copy(l, h, d, c).start()

                @pl.when((k > 0) & (k < n - 1))
                def _():
                    rs_copy(l, h, d, c).wait_recv()
                    rs_send[l, h, d, c] = (part[h, d, c] + rs_recv[l, h, d, c].astype(f32)).astype(jnp.bfloat16)
                    rs_copy(l, h, d, c).start()

                @pl.when(k == n - 1)
                def _():
                    rs_copy(l, h, d, c).wait_recv()
                    hidden(h, l, d, c)
                    ag_copy(l, h, d, c).start()
                    down(h, l, d, c)

        for d in range(2):
            j = n - 1 - me if d == 1 else me
            c = tau - head - SKEW_BACK * j

            @pl.when((j > 0) & (c >= 0) & (c < chunks))
            def _():
                ag_copy(l, h, d, c).wait_recv()

                @pl.when(j < n - 1)
                def _():
                    ag_copy(l, h, d, c).start()

                down(h, l, d, c)

        @pl.when(tau == t_term)
        def _():
            tbuf[l, h] = acc[h].astype(jnp.bfloat16)
            for o in range(1, m):
                t_copy(l, h, o).start()

        @pl.when(tau == t_own)
        def _():
            mine = own(mc)
            total = tbuf[l, h, mine].astype(f32)
            for o in range(1, m):
                t_copy(l, h, o).wait_recv()
                total = total + rbuf[l, h, o].astype(f32)
            snew[l, h, mine] = (0.5 * cur[h, mine].astype(f32) + total).astype(jnp.bfloat16)
            for o in range(1, m):
                n_copy(l, h, o).start()

        @pl.when(tau == t_back)
        def _():
            for o in range(1, m):
                n_wait(l, h, o)
            prep(h, l + 1, snew[l, h])

    for h in range(groups):
        prep(h, 0, s_in[h * rows : (h + 1) * rows])

    def body(t, carry):
        @pl.when(t == min(chunks - 1, head))
        def _():
            for l in range(layers):
                dcopy(l).start()
                if l + 1 < layers:
                    late(l + 1, 0).start()
                    late(l + 1, 1).start()

        for h in range(groups):
            at = t - h * lag

            @pl.when((at >= 0) & (at < layers * per_layer))
            def _():
                l = at // per_layer
                step(h, l, at - l * per_layer)

        return carry

    lax.fori_loop(0, layers * per_layer + (groups - 1) * lag, body, 0)

    for h in range(groups):
        finish_scale(h, layers)
        factor = jnp.concatenate([scale[h]] * (dl // LANES), axis=1)
        out[h * rows : (h + 1) * rows] = (
            cur[h].astype(f32) * factor * fg[...].astype(f32).reshape(1, dl)
        ).astype(jnp.bfloat16)

    def drain(i, carry):
        l = i // chunks
        c = i - l * chunks
        for h in range(groups):
            for d in range(2):
                k = me if d == 1 else n - 1 - me

                @pl.when(k < n - 1)
                def _():
                    rs_copy(l, h, d, c).wait_send()

                @pl.when(k > 0)
                def _():
                    ag_copy(l, h, d, c).wait_send()

        return carry

    lax.fori_loop(0, layers * chunks, drain, 0)
    for h in range(groups):
        for l in range(layers):
            for o in range(1, m):
                t_copy(l, h, o).wait_send()
                n_copy(l, h, o).wait_send()
        for l in range(layers + 1):
            for o in range(1, n):
                sq_copy(l, h, o).wait_send()


def body(n, m, width, stream, norm_gain, gate_weight, value_weight, gate_taps, value_taps,
         gate_bias, value_bias, down_weight, final_gain):
    batch, length, dl = stream.shape
    layers, _, ff = gate_weight.shape
    groups = GROUPS if batch % GROUPS == 0 else 1
    rows = batch * length // groups
    chunks = CHUNKS
    cw = ff // 2 // chunks
    bf16, f32 = jnp.bfloat16, jnp.float32
    vmem = pl.BlockSpec(memory_space=pltpu.VMEM)
    hbm = pl.BlockSpec(memory_space=pl.ANY)
    dma = pltpu.SemaphoreType.DMA
    result = pl.pallas_call(
        functools.partial(chain_kernel, (n, m, width, length)),
        out_shape=jax.ShapeDtypeStruct((batch * length, dl), bf16),
        in_specs=[vmem] * 7 + [hbm] * 3,
        out_specs=vmem,
        scratch_shapes=[
            pltpu.VMEM(gate_weight.shape, bf16),
            pltpu.VMEM(value_weight.shape, bf16),
            pltpu.VMEM(down_weight.shape, bf16),
            pltpu.VMEM((groups, rows, dl), bf16),
            pltpu.VMEM((groups, rows, dl), bf16),
            pltpu.VMEM((groups, 2, chunks, rows, 2 * cw), f32),
            pltpu.VMEM((layers, groups, 2, chunks, rows, 2 * cw), bf16),
            pltpu.VMEM((layers, groups, 2, chunks, rows, 2 * cw), bf16),
            pltpu.VMEM((layers, groups, 2, chunks, rows, cw), bf16),
            pltpu.VMEM((groups, rows, dl), f32),
            pltpu.VMEM((groups, rows, LANES), f32),
            pltpu.VMEM((layers + 1, groups, 8, LANES), f32),
            pltpu.VMEM((layers + 1, groups, n, 8, LANES), f32),
            pltpu.VMEM((layers, groups, rows, dl), bf16),
            pltpu.VMEM((layers, groups, m, rows // m, dl), bf16),
            pltpu.VMEM((layers, groups, rows, dl), bf16),
            dma((2, 2, chunks)),
            dma((2, layers)),
            dma((layers,)),
            dma((layers, groups, 2, chunks)),
            dma((layers, groups, 2, chunks)),
            dma((layers, groups, 2, chunks)),
            dma((layers, groups, 2, chunks)),
            dma((layers + 1, groups, n)),
            dma((layers + 1, groups, n)),
            dma((layers, groups, m)),
            dma((layers, groups, m)),
            dma((layers, groups, m)),
            dma((layers, groups, m)),
        ],
        compiler_params=pltpu.CompilerParams(
            collective_id=0, has_side_effects=True, vmem_limit_bytes=66_000_000
        ),
    )(
        stream.reshape(batch * length, dl), norm_gain, gate_taps.swapaxes(0, 1), value_taps.swapaxes(0, 1), gate_bias, value_bias,
        final_gain, gate_weight, value_weight, down_weight,
    )
    return result.reshape(batch, length, dl)


def solution(mesh):
    n, m = mesh.shape["ra"], mesh.shape["cb"]

    def run(stream, *rest):
        specs = (
            P("dp", None, "ra"),
            P(None, "ra"),
            P(None, "ra", "cb"),
            P(None, "ra", "cb"),
            P(None, None, "cb"),
            P(None, None, "cb"),
            P(None, "cb"),
            P(None, "cb"),
            P(None, "cb", "ra"),
            P("ra"),
        )
        return jax.shard_map(
            functools.partial(body, n, m, stream.shape[2]),
            mesh=mesh, in_specs=specs, out_specs=P("dp", None, "ra"), check_vma=False,
        )(stream, *rest)

    return run
```

profile of v0, /device:TPU:0, one launch (start us, length us, event | category | flops | bytes accessed | tf_op | source)
XLA Modules:
  0.0 106.7 jit_solution(3171239562146508453)
XLA Ops:
  0.0 105.0 %shard_map.100 = bf16[128,1024]{1,0:T(8,128)(2,1)} custom-call(bf16[128,1024]{1,0:T(8,128)(2,1)} %bitcast.5, bf16[2,1024]{1,0:T(2,128)(2,1)} %ng.1, bf16[3,2,3072]{2,1,0:T(2,128)(2,1)} %bitcast.6, bf16[3,2,3072]{2,1,0:T(2,128)(2,1)} %bitcast.7, bf16[2,3072]{1,0:T(2,128)(2,1)} %gb.1, bf16[2,3072]{1,0:T(2,128)(2,1)} %vb.1, bf16[1024]{0:T(1024)(128)(2,1)} %fg.1, ...), custom_call_target="tpu_custom_call" | custom-call | tf_op jit(solution)/shard_map/pallas_call | solution.py:328
  105.0 1.7 %copy.12 = bf16[2,64,1024]{2,1,0:T(8,128)(2,1)} copy(bf16[2,64,1024]{2,1,0:T(8,128)(2,1)} %bitcast.4) | data formatting | bytes 524288
where the time goes:
time: 107 us
  Pallas kernels  105 us (98%)
  local copies, waits for them, and re-layouts  1.67 us (2%)
    pallas_call x1, Pallas kernels, body(): pl.pallas_call(functools.partial(chain_kernel, (n, m, width, length)), ou...  105 us

commit v1 on v0

v1 whole, which is shorter than its diff:
```python
import functools

import jax
import jax.numpy as jnp
from jax import lax
from jax.experimental import pallas as pl
from jax.experimental.pallas import tpu as pltpu
from jax.sharding import PartitionSpec as P

EPS = 1e-06
MESH = pl.DeviceIdType.MESH
LANES = 128
UNITS = 256
SKEW = 3
SKEW_BACK = 2
OWN_LAG = 3
NEXT_LAG = 7
END_LAG = 3
UP, MIX = 0, 1


def chain_kernel(
    dims,
    s_in, ng, gt, vt, gb, vb, fg, wg_hbm, wv_hbm, dn_hbm,
    out,
    w, dn, u, part, rs_send, rs_recv, hid, acc, scale, coef,
    sq_send, sq_recv, tbuf, rbuf, snew, sfin, fsq_send, fsq_recv, fin,
    wsem, dsem, p_ss, p_rs, rs_ss, rs_rs, ag_ss, ag_rs, sq_ss, sq_rs,
    t_ss, t_rs, n_ss, n_rs, i_ss, i_rs, fs_ss, fs_rs, f_ss, f_rs,
):
    n, m, width = dims
    layers, _, chunks, dl, cw2 = w.shape
    cw = cw2 // 2
    groups, rows = hid.shape[1], hid.shape[4]
    half = groups // 2
    rq = rows // m
    taps = gt.shape[0]
    me = lax.axis_index("ra")
    mc = lax.axis_index("cb")
    core = lax.axis_index("dp")
    f32, bf16 = jnp.float32, jnp.bfloat16
    items = groups * chunks
    off_owner = SKEW * (n - 2)
    off_down = off_owner + SKEW_BACK * (n - 1)
    off_own = off_down + OWN_LAG
    off_end = off_own + END_LAG
    period = max(items, chunks + off_own + NEXT_LAG)

    def place(lane):
        return jnp.where(lane == 1, me, n - 1 - me)

    def wcopy(l, lane, c, which):
        src = (wg_hbm, wv_hbm)[which]
        cols = pl.ds(pl.multiple_of((lane * chunks + c) * cw, LANES), cw)
        return pltpu.make_async_copy(
            src.at[l, :, cols], w.at[l, lane, c, :, pl.ds(which * cw, cw)], wsem.at[l, lane, c, which]
        )

    def dcopy(l, lane, c):
        units = pl.ds(pl.multiple_of((lane * chunks + c) * cw, LANES), cw)
        return pltpu.make_async_copy(dn_hbm.at[l, units, :], dn.at[l, lane, c], dsem.at[l, lane, c])

    def remote(src, dst, ss, rs, **to):
        return pltpu.make_async_remote_copy(
            src_ref=src, dst_ref=dst, send_sem=ss, recv_sem=rs, device_id=to, device_id_type=MESH
        )

    def toward(lane, back):
        step = jnp.where((lane == 1) != back, 1, n - 1)
        return lax.rem(me + step, n)

    def own(q):
        return pl.ds(pl.multiple_of(q * rq, rq), rq)

    def part_copy(l, h, lane, c):
        return remote(
            part.at[h, lane, c], part.at[h, lane, c], p_ss.at[l, h, lane, c], p_rs.at[l, h, lane, c], dp=MIX
        )

    def rs_copy(l, h, lane, c):
        return remote(
            rs_send.at[l, h, lane, c], rs_recv.at[l, h, lane, c],
            rs_ss.at[l, h, lane, c], rs_rs.at[l, h, lane, c], ra=toward(lane, False), dp=MIX,
        )

    def ag_copy(l, h, lane, c):
        return remote(
            hid.at[l, h, lane, c], hid.at[l, h, lane, c],
            ag_ss.at[l, h, lane, c], ag_rs.at[l, h, lane, c], ra=toward(lane, True), dp=MIX,
        )

    def sq_copy(l, h, e):
        return remote(
            sq_send.at[l, h], sq_recv.at[l, h, me], sq_ss.at[l, h, e], sq_rs.at[l, h, me],
            ra=(0, n - 1)[e], dp=MIX,
        )

    def sq_wait(l, h, r):
        remote(
            sq_send.at[l, h], sq_recv.at[l, h, r], sq_ss.at[l, h, 0], sq_rs.at[l, h, r], ra=me, dp=MIX
        ).wait_recv()

    def t_copy(l, h, o):
        to = lax.rem(mc + o, m)
        return remote(tbuf.at[l, h, own(to)], rbuf.at[l, h, o], t_ss.at[l, h, o], t_rs.at[l, h, o], cb=to)

    def n_copy(l, h, o):
        mine = own(mc)
        return remote(
            snew.at[l, h, mine], snew.at[l, h, mine], n_ss.at[l, h, o], n_rs.at[l, h, o],
            cb=lax.rem(mc + o, m), dp=UP,
        )

    def n_wait(l, h, o):
        theirs = own(lax.rem(mc + m - o, m))
        remote(
            snew.at[l, h, theirs], snew.at[l, h, theirs], n_ss.at[l, h, o], n_rs.at[l, h, o],
            cb=lax.rem(mc + o, m), dp=UP,
        ).wait_recv()

    def full_copy(h):
        return remote(
            s_in.at[pl.ds((h - half) * rows, rows)], snew.at[0, h], i_ss.at[h], i_rs.at[h], dp=UP
        )

    def mine_copy(h):
        return remote(
            s_in.at[pl.ds(pl.multiple_of(h * rows + mc * rq, rq), rq)], snew.at[0, h, own(mc)],
            i_ss.at[h], i_rs.at[h], dp=MIX,
        )

    def fsq_copy(h, o):
        return remote(
            fsq_send.at[h], fsq_recv.at[h, o], fs_ss.at[h, o], fs_rs.at[h, o], ra=lax.rem(me + o, n)
        )

    def out_rows(h, q):
        return pl.ds(pl.multiple_of(lax.rem(h, half) * rows + q * rq, rq), rq)

    def f_copy(h, o):
        return remote(
            fin.at[h], out.at[out_rows(h, mc)], f_ss.at[h, o], f_rs.at[h, o],
            cb=lax.rem(mc + o, m), dp=h // half,
        )

    def f_wait(h, o):
        remote(
            fin.at[h], out.at[out_rows(h, lax.rem(mc + m - o, m))], f_ss.at[h, o], f_rs.at[h, o],
            cb=lax.rem(mc + o, m), dp=h // half,
        ).wait_recv()

    @pl.when(core == UP)
    def _():
        for c in range(chunks):
            for lane in range(2):
                for which in range(2):
                    wcopy(0, lane, c, which).start()

    @pl.when(core == MIX)
    def _():
        for c in range(chunks):
            for lane in range(2):
                dcopy(0, lane, c).start()

    barrier = pltpu.get_barrier_semaphore()
    for o in range(n):
        for other in range(2):
            if o or other:
                pl.semaphore_signal(
                    barrier, inc=1, device_id={"ra": lax.rem(me + o, n), "dp": lax.rem(core + other, 2)},
                    device_id_type=MESH,
                )
    for o in range(1, m):
        for other in range(2):
            pl.semaphore_signal(
                barrier, inc=1, device_id={"cb": lax.rem(mc + o, m), "dp": lax.rem(core + other, 2)},
                device_id_type=MESH,
            )

    @pl.when(core == UP)
    def _():
        for h in range(half):
            snew[0, h] = s_in[h * rows : (h + 1) * rows]

    @pl.when(core == MIX)
    def _():
        mine = own(mc)
        for h in range(half, groups):
            snew[0, h, mine] = s_in[pl.ds(pl.multiple_of((h - half) * rows + mc * rq, rq), rq)]
        acc[...] = jnp.zeros(acc.shape, f32)
        lane = jnp.where(me == 0, 0, 1)
        for l in range(layers):
            for c in range(chunks):
                cols = pl.ds(pl.multiple_of((lane * chunks + c) * cw, LANES), cw)
                for i in range(taps):
                    coef[l, c, i : i + 1] = gt[i, l : l + 1, cols].astype(f32)
                    coef[l, c, taps + 1 + i : taps + 2 + i] = vt[i, l : l + 1, cols].astype(f32)
                coef[l, c, taps : taps + 1] = gb[l : l + 1, cols].astype(f32)
                coef[l, c, 2 * taps + 1 : 2 * taps + 2] = vb[l : l + 1, cols].astype(f32)

    pl.semaphore_wait(barrier, 2 * n - 1 + 2 * (m - 1))

    @pl.when(core == UP)
    def _():
        for h in range(half):
            mine_copy(h).start()

        first = jnp.where(me == 0, 1, 0)

        def item(i, carry):
            l = i // items
            rest = i - l * items
            h = rest // chunks
            c = rest - h * chunks

            @pl.when(c == 0)
            def _():
                @pl.when((l == 0) & (h >= half))
                def _():
                    full_copy(h).wait_recv()

                @pl.when(l > 0)
                def _():
                    for o in range(m):
                        n_wait(l, h, o)

                gain = ng[0:1, :].astype(f32)
                for x in range(1, layers):
                    gain = jnp.where(l == x, ng[x : x + 1, :].astype(f32), gain)
                u[...] = (snew[l, h].astype(f32) * gain).astype(bf16)

            @pl.when(h == 0)
            def _():
                for lane in range(2):
                    for which in range(2):
                        wcopy(l, lane, c, which).wait()

            for a in range(2):
                lane = first if a == 0 else 1 - first
                k = place(lane)

                def up():
                    return jnp.dot(u[...], w[l, lane, c], preferred_element_type=f32)

                if a == 0:

                    @pl.when(k == 0)
                    def _():
                        rs_send[l, h, lane, c] = up().astype(bf16)
                        rs_copy(l, h, lane, c).start()

                @pl.when(k > 0)
                def _():
                    @pl.when(l > 0)
                    def _():
                        part_copy(l - 1, h, lane, c).wait_send()

                    part[h, lane, c] = up()
                    part_copy(l, h, lane, c).start()

            @pl.when(c == 0)
            def _():
                values = snew[l, h].astype(f32)
                total = jnp.sum(values * values, axis=1, keepdims=True)
                square = jnp.broadcast_to(jnp.concatenate([total] * (LANES // rows), axis=0), (LANES, LANES))
                sq_send[l, h] = square.T[0:8]
                for e in range(2):
                    sq_copy(l, h, e).start()

            @pl.when(i == chunks - 1)
            def _():
                for x in range(1, layers):
                    for cc in range(chunks):
                        for lane in range(2):
                            for which in range(2):
                                wcopy(x, lane, cc, which).start()

            return carry

        lax.fori_loop(0, layers * items, item, 0)

        for h in range(half):
            for o in range(m):
                f_wait(h, o)

        def drain(i, carry):
            l = i // items
            rest = i - l * items
            h = rest // chunks
            c = rest - h * chunks
            for lane in range(2):
                k = place(lane)

                @pl.when(k == 0)
                def _():
                    rs_copy(l, h, lane, c).wait_send()

                @pl.when((k > 0) & (l == layers - 1))
                def _():
                    part_copy(l, h, lane, c).wait_send()

            return carry

        lax.fori_loop(0, layers * items, drain, 0)
        for h in range(half):
            mine_copy(h).wait_send()
        for l in range(layers):
            for h in range(groups):
                for e in range(2):
                    sq_copy(l, h, e).wait_send()

    @pl.when(core == MIX)
    def _():
        for h in range(half, groups):
            full_copy(h).start()

        position = lax.broadcasted_iota(jnp.int32, (rows, cw), 0)

        def mix(x, rest, at):
            result = rest[at + taps : at + taps + 1] + x * rest[at + taps - 1 : at + taps]
            for back in range(1, taps):
                moved = jnp.where(position >= back, pltpu.roll(x, back, 0), 0.0)
                result = result + moved * rest[at + taps - 1 - back : at + taps - back]
            return result

        def finish_scale(l, h):
            total = jnp.zeros((8, LANES), f32)
            for r in range(n):
                sq_wait(l, h, r)
                total = total + sq_recv[l, h, r]
            inverse = lax.rsqrt(total / width + EPS)
            scale[...] = jnp.broadcast_to(inverse[0:1], (LANES, LANES)).T[0:rows]

        def split(i):
            at = jnp.maximum(i, 0)
            l = at // period
            rest = at - l * period
            valid = (i >= 0) & (l < layers) & (rest < items)
            l = jnp.minimum(l, layers - 1)
            rest = jnp.minimum(rest, items - 1)
            h = rest // chunks
            return valid, l, h, rest - h * chunks

        def step(t, carry):
            for lane in range(2):
                k = place(lane)
                valid, l, h, c = split(t - SKEW * (k - 1))

                @pl.when(valid & (k > 0))
                def _():
                    part_copy(l, h, lane, c).wait_recv()
                    rs_copy(l, h, lane, c).wait_recv()

                    @pl.when(k < n - 1)
                    def _():
                        rs_send[l, h, lane, c] = (part[h, lane, c] + rs_recv[l, h, lane, c].astype(f32)).astype(bf16)
                        rs_copy(l, h, lane, c).start()

                    @pl.when(k == n - 1)
                    def _():
                        @pl.when(c == 0)
                        def _():
                            finish_scale(l, h)

                        factor = jnp.concatenate([scale[...]] * (cw // LANES), axis=1)
                        rest = coef[l, c]
                        gate = (part[h, lane, c, :, :cw] + rs_recv[l, h, lane, c, :, :cw].astype(f32)) * factor
                        value = (part[h, lane, c, :, cw:] + rs_recv[l, h, lane, c, :, cw:].astype(f32)) * factor
                        gate = mix(gate, rest, 0)
                        value = mix(value, rest, taps + 1)
                        hid[l, h, lane, c] = (jax.nn.gelu(gate) * value).astype(bf16)
                        ag_copy(l, h, lane, c).start()

            for lane in range(2):
                k = place(lane)
                valid, l, h, c = split(t - off_owner - SKEW_BACK * (n - 1 - k))

                @pl.when(valid & (k < n - 1))
                def _():
                    ag_copy(l, h, lane, c).wait_recv()

                    @pl.when(k > 0)
                    def _():
                        ag_copy(l, h, lane, c).start()

            valid, l, h, c = split(t - off_own)

            @pl.when(valid & (c == chunks - 1))
            def _():
                mine = own(mc)

                @pl.when((l == 0) & (h < half))
                def _():
                    mine_copy(h).wait_recv()

                total = tbuf[l, h, mine].astype(f32)
                for o in range(1, m):
                    t_copy(l, h, o).wait_recv()
                    total = total + rbuf[l, h, o].astype(f32)
                new = (0.5 * snew[l, h, mine].astype(f32) + total).astype(bf16)

                @pl.when(l < layers - 1)
                def _():
                    snew[l + 1, h, mine] = new
                    for o in range(m):
                        n_copy(l + 1, h, o).start()

                @pl.when(l == layers - 1)
                def _():
                    sfin[h] = new
                    values = new.astype(f32)
                    fsq_send[h] = jnp.broadcast_to(jnp.sum(values * values, axis=1, keepdims=True), (rq, LANES))
                    for o in range(1, n):
                        fsq_copy(h, o).start()

            valid, l, h, c = split(t - off_down)

            @pl.when(valid)
            def _():
                @pl.when(h == 0)
                def _():
                    for lane in range(2):
                        dcopy(l, lane, c).wait()

                acc[...] += jnp.dot(hid[l, h, 0, c], dn[l, 0, c], preferred_element_type=f32) + jnp.dot(
                    hid[l, h, 1, c], dn[l, 1, c], preferred_element_type=f32
                )

                @pl.when(c == chunks - 1)
                def _():
                    tbuf[l, h] = acc[...].astype(bf16)
                    for o in range(1, m):
                        t_copy(l, h, o).start()
                    acc[...] = jnp.zeros(acc.shape, f32)

            valid, l, h, c = split(t - off_end)

            @pl.when(valid & (c == chunks - 1) & (l == layers - 1))
            def _():
                total = fsq_send[h]
                for o in range(1, n):
                    fsq_copy(h, o).wait_recv()
                    total = total + fsq_recv[h, o]
                factor = jnp.concatenate([lax.rsqrt(total / width + EPS)] * (dl // LANES), axis=1)
                fin[h] = (sfin[h].astype(f32) * factor * fg[...].astype(f32).reshape(1, dl)).astype(bf16)

                @pl.when(h < half)
                def _():
                    f_copy(h, 0).start()

                for o in range(1, m):
                    f_copy(h, o).start()

                @pl.when(h >= half)
                def _():
                    out[out_rows(h, mc)] = fin[h]

            @pl.when(t == chunks - 1)
            def _():
                for x in range(1, layers):
                    for cc in range(chunks):
                        for lane in range(2):
                            dcopy(x, lane, cc).start()

            return carry

        lax.fori_loop(0, (layers - 1) * period + items + off_end, step, 0)

        for h in range(half, groups):
            for o in range(1, m):
                f_wait(h, o)

        def drain(i, carry):
            l = i // items
            rest = i - l * items
            h = rest // chunks
            c = rest - h * chunks
            for lane in range(2):
                k = place(lane)

                @pl.when((k > 0) & (k < n - 1))
                def _():
                    rs_copy(l, h, lane, c).wait_send()

                @pl.when(k > 0)
                def _():
                    ag_copy(l, h, lane, c).wait_send()

            return carry

        lax.fori_loop(0, layers * items, drain, 0)
        for h in range(half, groups):
            full_copy(h).wait_send()
        for h in range(groups):
            for l in range(layers):
                for o in range(1, m):
                    t_copy(l, h, o).wait_send()
                if l:
                    for o in range(m):
                        n_copy(l, h, o).wait_send()
            for o in range(1, n):
                fsq_copy(h, o).wait_send()
            for o in range(0 if h < half else 1, m):
                f_copy(h, o).wait_send()


def body(n, m, width, stream, norm_gain, gate_weight, value_weight, gate_taps, value_taps,
         gate_bias, value_bias, down_weight, final_gain):
    batch, length, dl = stream.shape
    layers, _, ff = gate_weight.shape
    taps = gate_taps.shape[1]
    groups, rows = 2 * batch, length
    cw = UNITS
    chunks = ff // 2 // cw
    rq = rows // m
    bf16, f32 = jnp.bfloat16, jnp.float32
    vmem = pl.BlockSpec(memory_space=pltpu.VMEM)
    hbm = pl.BlockSpec(memory_space=pl.ANY)
    dma = pltpu.SemaphoreType.DMA
    pieces = (layers, groups, 2, chunks)
    result = pl.pallas_call(
        functools.partial(chain_kernel, (n, m, width)),
        out_shape=jax.ShapeDtypeStruct((batch * length, dl), bf16),
        in_specs=[vmem] * 7 + [hbm] * 3,
        out_specs=vmem,
        scratch_shapes=[
            pltpu.VMEM((layers, 2, chunks, dl, 2 * cw), bf16),
            pltpu.VMEM((layers, 2, chunks, cw, dl), bf16),
            pltpu.VMEM((rows, dl), bf16),
            pltpu.VMEM((groups, 2, chunks, rows, 2 * cw), f32),
            pltpu.VMEM(pieces + (rows, 2 * cw), bf16),
            pltpu.VMEM(pieces + (rows, 2 * cw), bf16),
            pltpu.VMEM(pieces + (rows, cw), bf16),
            pltpu.VMEM((rows, dl), f32),
            pltpu.VMEM((rows, LANES), f32),
            pltpu.VMEM((layers, chunks, -(-(2 * taps + 2) // 8) * 8, cw), f32),
            pltpu.VMEM((layers, groups, 8, LANES), f32),
            pltpu.VMEM((layers, groups, n, 8, LANES), f32),
            pltpu.VMEM((layers, groups, rows, dl), bf16),
            pltpu.VMEM((layers, groups, m, rq, dl), bf16),
            pltpu.VMEM((layers, groups, rows, dl), bf16),
            pltpu.VMEM((groups, rq, dl), bf16),
            pltpu.VMEM((groups, rq, LANES), f32),
            pltpu.VMEM((groups, n, rq, LANES), f32),
            pltpu.VMEM((groups, rq, dl), bf16),
            dma((layers, 2, chunks, 2)),
            dma((layers, 2, chunks)),
            dma(pieces), dma(pieces), dma(pieces), dma(pieces), dma(pieces), dma(pieces),
            dma((layers, groups, 2)), dma((layers, groups, n)),
            dma((layers, groups, m)), dma((layers, groups, m)),
            dma((layers, groups, m)), dma((layers, groups, m)),
            dma((groups,)), dma((groups,)),
            dma((groups, n)), dma((groups, n)),
            dma((groups, m)), dma((groups, m)),
        ],
        compiler_params=pltpu.CompilerParams(
            collective_id=0, has_side_effects=True, vmem_limit_bytes=67_000_000
        ),
    )(
        stream.reshape(batch * length, dl), norm_gain, gate_taps.swapaxes(0, 1), value_taps.swapaxes(0, 1),
        gate_bias, value_bias, final_gain, gate_weight, value_weight, down_weight,
    )
    return result.reshape(batch, length, dl)


def solution(mesh):
    n, m = mesh.shape["ra"], mesh.shape["cb"]

    def run(stream, *rest):
        specs = (
            P("dp", None, "ra"),
            P(None, "ra"),
            P(None, "ra", "cb"),
            P(None, "ra", "cb"),
            P(None, None, "cb"),
            P(None, None, "cb"),
            P(None, "cb"),
            P(None, "cb"),
            P(None, "cb", "ra"),
            P("ra"),
        )
        return jax.shard_map(
            functools.partial(body, n, m, stream.shape[2]),
            mesh=mesh, in_specs=specs, out_specs=P("dp", None, "ra"), check_vma=False,
        )(stream, *rest)

    return run
```

time: 107 us -> 96.6 us (0.903)
  the two profiles are of different devices: /device:TPU:0 before, /device:TPU:1 now
where the time goes in v1:
time: 96.6 us; the launch traced here: 96.4 us
  Pallas kernels  94.8 us (98%)
  local copies, waits for them, and re-layouts  1.67 us (2%)
    pallas_call x1, Pallas kernels, body(): pl.pallas_call(functools.partial(chain_kernel, (n, m, width)), out_shape=...  94.8 us

profile of v1, /device:TPU:1, one launch (start us, length us, event | category | flops | bytes accessed | tf_op | source)
XLA Modules:
  0.0 96.4 jit_solution(12169977947276908357)
XLA Ops:
  0.0 94.8 %shard_map.100 = bf16[128,1024]{1,0:T(8,128)(2,1)} custom-call(bf16[128,1024]{1,0:T(8,128)(2,1)} %bitcast.5, bf16[2,1024]{1,0:T(2,128)(2,1)} %ng.1, bf16[3,2,3072]{2,1,0:T(2,128)(2,1)} %bitcast.6, bf16[3,2,3072]{2,1,0:T(2,128)(2,1)} %bitcast.7, bf16[2,3072]{1,0:T(2,128)(2,1)} %gb.1, bf16[2,3072]{1,0:T(2,128)(2,1)} %vb.1, bf16[1024]{0:T(1024)(128)(2,1)} %fg.1, ...), custom_call_target="tpu_custom_call" | custom-call | tf_op jit(solution)/shard_map/pallas_call | solution.py:521
  94.8 1.7 %copy.12 = bf16[2,64,1024]{2,1,0:T(8,128)(2,1)} copy(bf16[2,64,1024]{2,1,0:T(8,128)(2,1)} %bitcast.4) | data formatting | bytes 524288

commit v2 on v1

v2 whole, which is shorter than its diff:
```python
import functools

import jax
import jax.numpy as jnp
from jax import lax
from jax.experimental import pallas as pl
from jax.experimental.pallas import tpu as pltpu
from jax.sharding import PartitionSpec as P

EPS = 1e-06
MESH = pl.DeviceIdType.MESH
LANES = 128
UNITS = 256
SKEW = 3
SKEW_BACK = 2
OWN_LAG = 3
NEXT_LAG = 5
END_LAG = 4
LAST_BACK = 0
OWN_EXTRA = 1
UP, MIX = 0, 1


def chain_kernel(
    dims,
    s_in, ng, gt, vt, gb, vb, fg, wg_hbm, wv_hbm, dn_hbm,
    out,
    w, dn, u, part, rs_send, rs_recv, hid, acc, scale, coef,
    sq_send, sq_recv, tbuf, rbuf, snew, fin, raw, fsq_send, fsq_recv,
    wsem, dsem, p_ss, rs_ss, rs_rs, ag_ss, ag_rs, sq_ss, sq_rs,
    t_ss, t_rs, n_ss, n_rs, i_ss, i_rs, fs_ss, fs_rs, f_ss, f_rs,
):
    n, m, width = dims
    layers, chunks, _, dl, cw2 = w.shape
    cw = cw2 // 2
    groups, rows = hid.shape[1], hid.shape[4]
    half = groups // 2
    rq = rows // m
    taps = gt.shape[0]
    me = lax.axis_index("ra")
    mc = lax.axis_index("cb")
    core = lax.axis_index("dp")
    f32, bf16 = jnp.float32, jnp.bfloat16
    items = groups * chunks
    off_owner = SKEW * (n - 2)
    off_down = off_owner + SKEW_BACK * (n - 1)
    off_own = off_down + OWN_LAG
    off_end = off_own + END_LAG
    period = max(items + OWN_EXTRA, chunks + off_own + NEXT_LAG)

    def place(lane):
        return jnp.where(lane == 1, me, n - 1 - me)

    def wcopy(l, lane, c, which):
        src = (wg_hbm, wv_hbm)[which]
        cols = pl.ds(pl.multiple_of((lane * chunks + c) * cw, LANES), cw)
        return pltpu.make_async_copy(
            src.at[l, :, cols], w.at[l, c, lane, :, pl.ds(which * cw, cw)], wsem.at[l, c]
        )

    def dcopy(l, lane, c):
        units = pl.ds(pl.multiple_of((lane * chunks + c) * cw, LANES), cw)
        return pltpu.make_async_copy(dn_hbm.at[l, units, :], dn.at[l, c, lane], dsem.at[l, c])

    def remote(src, dst, ss, rs, **to):
        return pltpu.make_async_remote_copy(
            src_ref=src, dst_ref=dst, send_sem=ss, recv_sem=rs, device_id=to, device_id_type=MESH
        )

    def toward(lane, back):
        step = jnp.where((lane == 1) != back, 1, n - 1)
        return lax.rem(me + step, n)

    def own(q):
        return pl.ds(pl.multiple_of(q * rq, rq), rq)

    def part_copy(l, h, lane, c):
        return remote(
            part.at[h, lane, c], part.at[h, lane, c], p_ss.at[l, h, lane], rs_rs.at[h, lane, c], dp=MIX
        )

    def rs_copy(l, h, lane, c):
        return remote(
            rs_send.at[l, h, lane, c], rs_recv.at[l, h, lane, c],
            rs_ss.at[l, h, lane], rs_rs.at[h, lane, c], ra=toward(lane, False), dp=MIX,
        )

    def ag_copy(l, h, lane, c):
        return remote(
            hid.at[l, h, lane, c], hid.at[l, h, lane, c],
            ag_ss.at[l, h, lane], ag_rs.at[h, lane, c], ra=toward(lane, True), dp=MIX,
        )

    def sq_copy(l, h, e):
        return remote(
            sq_send.at[l, h], sq_recv.at[l, h, me], sq_ss.at[l, h, e], sq_rs.at[l, h],
            ra=(0, n - 1)[e], dp=MIX,
        )

    def t_copy(l, h, o):
        to = lax.rem(mc + o, m)
        return remote(tbuf.at[l, h, own(to)], rbuf.at[l, h, o], t_ss.at[l, h], t_rs.at[l, h], cb=to)

    def n_copy(l, h, o):
        mine = own(mc)
        return remote(
            snew.at[l, h, mine], snew.at[l, h, mine], n_ss.at[l, h], n_rs.at[l, h],
            cb=lax.rem(mc + o, m), dp=UP,
        )

    def full_copy(h):
        return remote(
            s_in.at[pl.ds((h - half) * rows, rows)], snew.at[0, h], i_ss.at[h], i_rs.at[h], dp=UP
        )

    def mine_copy(h):
        return remote(
            s_in.at[pl.ds(pl.multiple_of(h * rows + mc * rq, rq), rq)], snew.at[0, h, own(mc)],
            i_ss.at[h], i_rs.at[h], dp=MIX,
        )

    def fsq_copy(h, r, o):
        return remote(
            fsq_send.at[h], fsq_recv.at[lax.rem(h, half), me * m + mc], fs_ss.at[h], fs_rs.at[h],
            ra=lax.rem(me + r, n), cb=lax.rem(mc + o, m), dp=h // half,
        )

    def f_copy(h, o):
        return remote(
            fin.at[h], raw.at[lax.rem(h, half), own(mc)], f_ss.at[h], f_rs.at[h],
            cb=lax.rem(mc + o, m), dp=h // half,
        )

    def arrived(ref, sem):
        remote(ref, ref, f_ss.at[0], sem, dp=core).wait_recv()

    def left(ref, sem):
        remote(ref, ref, sem, f_rs.at[0], dp=core).wait_send()

    def end(h):
        at = lax.rem(h, half)
        for q in range(m):
            total = fsq_recv[at, q]
            for r in range(1, n):
                total = total + fsq_recv[at, r * m + q]
            inverse = lax.rsqrt(total / width + EPS)
            factor = jnp.broadcast_to(inverse, (LANES, LANES)).T[0:rq]
            factor = jnp.concatenate([factor] * (dl // LANES), axis=1)
            scaled = raw[at, q * rq : (q + 1) * rq].astype(f32) * factor * fg[...].astype(f32).reshape(1, dl)
            out[pl.ds(pl.multiple_of(at * rows + q * rq, rq), rq)] = scaled.astype(bf16)

    barrier = pltpu.get_barrier_semaphore()

    def greet(**to):
        pl.semaphore_signal(barrier, inc=1, device_id=to, device_id_type=MESH)

    @pl.when(core == UP)
    def _():
        for o in range(m):
            greet(cb=lax.rem(mc + o, m), dp=MIX)

    @pl.when(core == MIX)
    def _():
        for o in range(n):
            greet(ra=lax.rem(me + o, n), dp=UP)
        for o in range(1, n):
            greet(ra=lax.rem(me + o, n), dp=MIX)
        for o in range(1, m):
            greet(cb=lax.rem(mc + o, m), dp=MIX)

    @pl.when(core == UP)
    def _():
        for c in range(chunks):
            for lane in range(2):
                for which in range(2):
                    wcopy(0, lane, c, which).start()

    @pl.when(core == MIX)
    def _():
        for c in range(chunks):
            for lane in range(2):
                dcopy(0, lane, c).start()

    @pl.when(core == UP)
    def _():
        for h in range(half):
            snew[0, h] = s_in[h * rows : (h + 1) * rows]

    @pl.when(core == MIX)
    def _():
        mine = own(mc)
        for h in range(half, groups):
            snew[0, h, mine] = s_in[pl.ds(pl.multiple_of((h - half) * rows + mc * rq, rq), rq)]
        acc[...] = jnp.zeros(acc.shape, f32)
        lane = jnp.where(me == 0, 0, 1)
        for l in range(layers):
            for c in range(chunks):
                cols = pl.ds(pl.multiple_of((lane * chunks + c) * cw, LANES), cw)
                for i in range(taps):
                    coef[l, c, i : i + 1] = gt[i, l : l + 1, cols].astype(f32)
                    coef[l, c, taps + 1 + i : taps + 2 + i] = vt[i, l : l + 1, cols].astype(f32)
                coef[l, c, taps : taps + 1] = gb[l : l + 1, cols].astype(f32)
                coef[l, c, 2 * taps + 1 : 2 * taps + 2] = vb[l : l + 1, cols].astype(f32)

    @pl.when(core == UP)
    def _():
        pl.semaphore_wait(barrier, n)
        for h in range(half):
            mine_copy(h).start()

        first = jnp.where(me == 0, 1, 0)

        def item(i, carry):
            l = i // items
            rest = i - l * items
            h = rest // chunks
            c = rest - h * chunks

            @pl.when(c == 0)
            def _():
                @pl.when((l == 0) & (h >= half))
                def _():
                    full_copy(h).wait_recv()

                @pl.when(l > 0)
                def _():
                    arrived(snew.at[l, h], n_rs.at[l, h])

                gain = ng[0:1, :].astype(f32)
                for x in range(1, layers):
                    gain = jnp.where(l == x, ng[x : x + 1, :].astype(f32), gain)
                u[...] = (snew[l, h].astype(f32) * gain).astype(bf16)

            @pl.when(h == 0)
            def _():
                pltpu.make_async_copy(w.at[l, c], w.at[l, c], wsem.at[l, c]).wait()

            for a in range(2):
                lane = first if a == 0 else 1 - first
                k = place(lane)

                def up():
                    return jnp.dot(u[...], w[l, c, lane], preferred_element_type=f32)

                if a == 0:

                    @pl.when(k == 0)
                    def _():
                        rs_send[l, h, lane, c] = up().astype(bf16)
                        rs_copy(l, h, lane, c).start()

                @pl.when(k > 0)
                def _():
                    @pl.when((l > 0) & (c == 0))
                    def _():
                        left(part.at[h, lane], p_ss.at[l - 1, h, lane])

                    part[h, lane, c] = up()
                    part_copy(l, h, lane, c).start()

            @pl.when(c == 0)
            def _():
                values = snew[l, h].astype(f32)
                total = jnp.sum(values * values, axis=1, keepdims=True)
                square = jnp.broadcast_to(jnp.concatenate([total] * (LANES // rows), axis=0), (LANES, LANES))
                sq_send[l, h] = square.T[0:8]
                for e in range(2):
                    sq_copy(l, h, e).start()

            @pl.when(i == chunks - 1)
            def _():
                for x in range(1, layers):
                    for cc in range(chunks):
                        for lane in range(2):
                            for which in range(2):
                                wcopy(x, lane, cc, which).start()

            return carry

        lax.fori_loop(0, layers * items, item, 0)

        for h in range(groups):
            for lane in range(2):
                k = place(lane)

                @pl.when(k == 0)
                def _():
                    for l in range(layers):
                        left(rs_send.at[l, h, lane], rs_ss.at[l, h, lane])

                @pl.when(k > 0)
                def _():
                    left(part.at[h, lane], p_ss.at[layers - 1, h, lane])

            for l in range(layers):
                for e in range(2):
                    sq_copy(l, h, e).wait_send()
        for h in range(half):
            mine_copy(h).wait_send()
        for h in range(half):
            arrived(raw.at[h], f_rs.at[h])
            arrived(fsq_recv.at[h], fs_rs.at[h])
            end(h)

    @pl.when(core == MIX)
    def _():
        pl.semaphore_wait(barrier, n + 2 * m - 2)
        for h in range(half, groups):
            full_copy(h).start()

        position = lax.broadcasted_iota(jnp.int32, (rows, cw), 0)

        def mix(x, rest, at):
            result = rest[at + taps : at + taps + 1] + x * rest[at + taps - 1 : at + taps]
            for back in range(1, taps):
                moved = jnp.where(position >= back, pltpu.roll(x, back, 0), 0.0)
                result = result + moved * rest[at + taps - 1 - back : at + taps - back]
            return result

        def finish_scale(l, h):
            arrived(sq_recv.at[l, h], sq_rs.at[l, h])
            total = jnp.zeros((8, LANES), f32)
            for r in range(n):
                total = total + sq_recv[l, h, r]
            inverse = lax.rsqrt(total / width + EPS)
            scale[...] = jnp.broadcast_to(inverse[0:1], (LANES, LANES)).T[0:rows]

        def split(i):
            at = jnp.maximum(i, 0)
            l = at // period
            rest = at - l * period
            valid = (i >= 0) & (l < layers) & (rest < items)
            l = jnp.minimum(l, layers - 1)
            rest = jnp.minimum(rest, items - 1)
            h = rest // chunks
            return valid, l, h, rest - h * chunks

        def later(i):
            last = (layers - 1) * period
            return jnp.where(i < last, i, jnp.where(i < last + LAST_BACK, -1, i - LAST_BACK))

        def step(t, carry):
            for lane in range(2):
                k = place(lane)
                valid, l, h, c = split(t - SKEW * (k - 1))

                @pl.when(valid & (k > 0))
                def _():
                    arrived(rs_recv.at[l, h, lane, 0:3], rs_rs.at[h, lane, c])

                    @pl.when(k < n - 1)
                    def _():
                        rs_send[l, h, lane, c] = (part[h, lane, c] + rs_recv[l, h, lane, c].astype(f32)).astype(bf16)
                        rs_copy(l, h, lane, c).start()

                    @pl.when(k == n - 1)
                    def _():
                        @pl.when(c == 0)
                        def _():
                            finish_scale(l, h)

                        factor = jnp.concatenate([scale[...]] * (cw // LANES), axis=1)
                        rest = coef[l, c]
                        gate = (part[h, lane, c, :, :cw] + rs_recv[l, h, lane, c, :, :cw].astype(f32)) * factor
                        value = (part[h, lane, c, :, cw:] + rs_recv[l, h, lane, c, :, cw:].astype(f32)) * factor
                        gate = mix(gate, rest, 0)
                        value = mix(value, rest, taps + 1)
                        hid[l, h, lane, c] = (jax.nn.gelu(gate) * value).astype(bf16)
                        ag_copy(l, h, lane, c).start()

            for lane in range(2):
                k = place(lane)
                valid, l, h, c = split(later(t - off_owner - SKEW_BACK * (n - 1 - k)))

                @pl.when(valid & (k < n - 1))
                def _():
                    ag_copy(l, h, lane, c).wait_recv()

                    @pl.when(k > 0)
                    def _():
                        ag_copy(l, h, lane, c).start()

            i = jnp.maximum(later(t - off_own), 0)
            l = i // period
            rest = i - l * period
            tardy = jnp.where(l < layers - 1, OWN_EXTRA, 0)
            fires = jnp.where(
                rest < items - 1, lax.rem(rest, chunks) == chunks - 1, rest == items - 1 + tardy
            )
            h = jnp.minimum(rest // chunks, groups - 1)

            @pl.when(fires & (l < layers))
            def _():
                mine = own(mc)

                @pl.when((l == 0) & (h < half))
                def _():
                    mine_copy(h).wait_recv()

                arrived(rbuf.at[l, h, 1:m], t_rs.at[l, h])
                total = tbuf[l, h, mine].astype(f32)
                for o in range(1, m):
                    total = total + rbuf[l, h, o].astype(f32)
                new = (0.5 * snew[l, h, mine].astype(f32) + total).astype(bf16)

                @pl.when(l < layers - 1)
                def _():
                    snew[l + 1, h, mine] = new
                    for o in range(m):
                        n_copy(l + 1, h, o).start()

                @pl.when(l == layers - 1)
                def _():
                    fin[h] = new
                    for o in range(1, m):
                        f_copy(h, o).start()
                    values = new.astype(f32)
                    square = jnp.sum(values * values, axis=1, keepdims=True)
                    square = jnp.broadcast_to(jnp.concatenate([square] * (LANES // rq), axis=0), (LANES, LANES))
                    fsq_send[h] = square.T[0:1]

                    @pl.when(h < half)
                    def _():
                        f_copy(h, 0).start()
                        fsq_copy(h, 0, 0).start()

                    @pl.when(h >= half)
                    def _():
                        raw[h - half, mine] = new
                        fsq_recv[h - half, me * m + mc] = fsq_send[h]

                    for o in range(1, m):
                        fsq_copy(h, 0, o).start()

                    def spread(r, carry):
                        for o in range(m):
                            fsq_copy(h, r, o).start()
                        return carry

                    lax.fori_loop(1, n, spread, 0)

            valid, l, h, c = split(later(t - off_down))

            @pl.when(valid)
            def _():
                @pl.when(h == 0)
                def _():
                    pltpu.make_async_copy(dn.at[l, c], dn.at[l, c], dsem.at[l, c]).wait()

                acc[...] += jnp.dot(hid[l, h, 0, c], dn[l, c, 0], preferred_element_type=f32) + jnp.dot(
                    hid[l, h, 1, c], dn[l, c, 1], preferred_element_type=f32
                )

                @pl.when(c == chunks - 1)
                def _():
                    tbuf[l, h] = acc[...].astype(bf16)
                    for o in range(1, m):
                        t_copy(l, h, o).start()
                    acc[...] = jnp.zeros(acc.shape, f32)
                    for lane in range(2):
                        k = place(lane)

                        @pl.when((k > 0) & (k < n - 1))
                        def _():
                            left(rs_send.at[l, h, lane], rs_ss.at[l, h, lane])

                        @pl.when(k > 0)
                        def _():
                            left(hid.at[l, h, lane], ag_ss.at[l, h, lane])

            valid, l, h, c = split(later(t - off_end))

            @pl.when(valid & (c == chunks - 1) & (l == layers - 1) & (h >= half))
            def _():
                at = h - half
                arrived(raw.at[at, 0 : rows - rq], f_rs.at[h])
                arrived(fsq_recv.at[at, 1 : n * m], fs_rs.at[h])
                end(h)

            @pl.when(t == chunks - 1)
            def _():
                for x in range(1, layers):
                    for cc in range(chunks):
                        for lane in range(2):
                            dcopy(x, lane, cc).start()

            return carry

        lax.fori_loop(0, (layers - 1) * period + items + off_end + LAST_BACK, step, 0)

        for h in range(half, groups):
            full_copy(h).wait_send()
        for h in range(groups):
            for l in range(layers):
                left(tbuf.at[l, h, 0 : rows - rq], t_ss.at[l, h])
                if l:
                    left(snew.at[l, h], n_ss.at[l, h])
            home = h // half
            left(raw.at[0, 0 : rows - home * rq], f_ss.at[h])
            left(fsq_recv.at[0, home : n * m], fs_ss.at[h])


def body(n, m, width, stream, norm_gain, gate_weight, value_weight, gate_taps, value_taps,
         gate_bias, value_bias, down_weight, final_gain):
    batch, length, dl = stream.shape
    layers, _, ff = gate_weight.shape
    taps = gate_taps.shape[1]
    groups, rows = 2 * batch, length
    cw = UNITS
    chunks = ff // 2 // cw
    rq = rows // m
    bf16, f32 = jnp.bfloat16, jnp.float32
    vmem = pl.BlockSpec(memory_space=pltpu.VMEM)
    hbm = pl.BlockSpec(memory_space=pl.ANY)
    dma = pltpu.SemaphoreType.DMA
    pieces = (layers, groups, 2, chunks)
    result = pl.pallas_call(
        functools.partial(chain_kernel, (n, m, width)),
        out_shape=jax.ShapeDtypeStruct((batch * length, dl), bf16),
        in_specs=[vmem] * 7 + [hbm] * 3,
        out_specs=vmem,
        scratch_shapes=[
            pltpu.VMEM((layers, chunks, 2, dl, 2 * cw), bf16),
            pltpu.VMEM((layers, chunks, 2, cw, dl), bf16),
            pltpu.VMEM((rows, dl), bf16),
            pltpu.VMEM((groups, 2, chunks, rows, 2 * cw), f32),
            pltpu.VMEM(pieces + (rows, 2 * cw), bf16),
            pltpu.VMEM(pieces + (rows, 2 * cw), bf16),
            pltpu.VMEM(pieces + (rows, cw), bf16),
            pltpu.VMEM((rows, dl), f32),
            pltpu.VMEM((rows, LANES), f32),
            pltpu.VMEM((layers, chunks, -(-(2 * taps + 2) // 8) * 8, cw), f32),
            pltpu.VMEM((layers, groups, 8, LANES), f32),
            pltpu.VMEM((layers, groups, n, 8, LANES), f32),
            pltpu.VMEM((layers, groups, rows, dl), bf16),
            pltpu.VMEM((layers, groups, m, rq, dl), bf16),
            pltpu.VMEM((layers, groups, rows, dl), bf16),
            pltpu.VMEM((groups, rq, dl), bf16),
            pltpu.VMEM((groups // 2, rows, dl), bf16),
            pltpu.VMEM((groups, 1, LANES), f32),
            pltpu.VMEM((groups // 2, n * m, 1, LANES), f32),
            dma((layers, chunks)),
            dma((layers, chunks)),
            dma(pieces[:3]), dma(pieces[:3]), dma(pieces[1:]), dma(pieces[:3]), dma(pieces[1:]),
            dma((layers, groups, 2)), dma((layers, groups)),
            dma((layers, groups)), dma((layers, groups)),
            dma((layers, groups)), dma((layers, groups)),
            dma((groups,)), dma((groups,)),
            dma((groups,)), dma((groups,)),
            dma((groups,)), dma((groups,)),
        ],
        compiler_params=pltpu.CompilerParams(
            collective_id=0, has_side_effects=True, vmem_limit_bytes=67_000_000
        ),
    )(
        stream.reshape(batch * length, dl), norm_gain, gate_taps.swapaxes(0, 1), value_taps.swapaxes(0, 1),
        gate_bias, value_bias, final_gain, gate_weight, value_weight, down_weight,
    )
    return result.reshape(batch, length, dl)


def solution(mesh):
    n, m = mesh.shape["ra"], mesh.shape["cb"]

    def run(stream, *rest):
        specs = (
            P("dp", None, "ra"),
            P(None, "ra"),
            P(None, "ra", "cb"),
            P(None, "ra", "cb"),
            P(None, None, "cb"),
            P(None, None, "cb"),
            P(None, "cb"),
            P(None, "cb"),
            P(None, "cb", "ra"),
            P("ra"),
        )
        return jax.shard_map(
            functools.partial(body, n, m, stream.shape[2]),
            mesh=mesh, in_specs=specs, out_specs=P("dp", None, "ra"), check_vma=False,
        )(stream, *rest)

    return run
```

time: 96.6 us -> 87.6 us (0.907)
  Pallas kernels: 94.8 us -> 85.8 us
    pallas_call x1, Pallas kernels: 94.8 us -> 85.8 us  [body(): pl.pallas_call(functools.partial(chain_kernel, (n, m, width)), out_shape=...]
where the time goes in v2:
time: 87.6 us; the launch traced here: 87.5 us
  Pallas kernels  85.8 us (98%)
  local copies, waits for them, and re-layouts  1.67 us (2%)
    pallas_call x1, Pallas kernels, body(): pl.pallas_call(functools.partial(chain_kernel, (n, m, width)), out_shape=...  85.8 us

profile of v2, /device:TPU:1, one launch (start us, length us, event | category | flops | bytes accessed | tf_op | source)
XLA Modules:
  0.0 87.5 jit_solution(5848793759602085896)
XLA Ops:
  0.0 85.8 %shard_map.100 = bf16[128,1024]{1,0:T(8,128)(2,1)} custom-call(bf16[128,1024]{1,0:T(8,128)(2,1)} %bitcast.5, bf16[2,1024]{1,0:T(2,128)(2,1)} %ng.1, bf16[3,2,3072]{2,1,0:T(2,128)(2,1)} %bitcast.6, bf16[3,2,3072]{2,1,0:T(2,128)(2,1)} %bitcast.7, bf16[2,3072]{1,0:T(2,128)(2,1)} %gb.1, bf16[2,3072]{1,0:T(2,128)(2,1)} %vb.1, bf16[1024]{0:T(1024)(128)(2,1)} %fg.1, ...), custom_call_target="tpu_custom_call" | custom-call | tf_op jit(solution)/shard_map/pallas_call | solution.py:517
  85.8 1.7 %copy.12 = bf16[2,64,1024]{2,1,0:T(8,128)(2,1)} copy(bf16[2,64,1024]{2,1,0:T(8,128)(2,1)} %bitcast.4) | data formatting | bytes 524288

commit v3 on v2

--- a/solution.py
+++ b/solution.py
@@ -12,25 +12,35 @@
 LANES = 128
 UNITS = 256
 SKEW = 3
-SKEW_BACK = 2
+SKEW_BACK = 3
 OWN_LAG = 3
-NEXT_LAG = 5
-END_LAG = 4
-LAST_BACK = 0
-OWN_EXTRA = 1
+NEXT_LAG = 7
+TUNED_FOR = (4, 6)
+SUMS = [0, 6, 13, 20, 31, 37, 44, 50]
+BACKS = [6, 13, 19, 25, 37, 43, 51, 57]
+OWNS = [24, 30, 36, 42, 59, 68, 72, 73]
 UP, MIX = 0, 1
 
 
 def chain_kernel(
     dims,
-    s_in, ng, gt, vt, gb, vb, fg, wg_hbm, wv_hbm, dn_hbm,
+    *refs,
+):
+    ins, (out, s_in, ng, gt, vt, gb, vb, fg), rest = refs[:7], refs[10:18], refs[18:]
+    (wg_hbm, wv_hbm, dn_hbm), held = refs[7:10], refs[11:18]
+    return chain(dims, ins, held, wg_hbm, wv_hbm, dn_hbm, out, *rest)
+
+
+def chain(
+    dims, ins, held, wg_hbm, wv_hbm, dn_hbm,
     out,
     w, dn, u, part, rs_send, rs_recv, hid, acc, scale, coef,
     sq_send, sq_recv, tbuf, rbuf, snew, fin, raw, fsq_send, fsq_recv,
-    wsem, dsem, p_ss, rs_ss, rs_rs, ag_ss, ag_rs, sq_ss, sq_rs,
+    wsem, dsem, xsem, p_ss, rs_ss, rs_rs, ag_ss, ag_rs, sq_ss, sq_rs,
     t_ss, t_rs, n_ss, n_rs, i_ss, i_rs, fs_ss, fs_rs, f_ss, f_rs,
 ):
     n, m, width = dims
+    s_in, ng, gt, vt, gb, vb, fg = held
     layers, chunks, _, dl, cw2 = w.shape
     cw = cw2 // 2
     groups, rows = hid.shape[1], hid.shape[4]
@@ -44,9 +54,14 @@
     items = groups * chunks
     off_owner = SKEW * (n - 2)
     off_down = off_owner + SKEW_BACK * (n - 1)
-    off_own = off_down + OWN_LAG
-    off_end = off_own + END_LAG
-    period = max(items + OWN_EXTRA, chunks + off_own + NEXT_LAG)
+    period = max(items, chunks + off_down + OWN_LAG + NEXT_LAG)
+    sums = [l * period + h * chunks for l in range(layers) for h in range(groups)]
+    backs = [x + off_owner for x in sums]
+    owns = [x + chunks - 1 + off_down + OWN_LAG for x in sums]
+    if (n, chunks) == TUNED_FOR and len(sums) == len(SUMS):
+        sums, backs, owns = SUMS, BACKS, OWNS
+    begin = min(sums)
+    finish = max(owns) + 1 + half
 
     def place(lane):
         return jnp.where(lane == 1, me, n - 1 - me)
@@ -55,12 +70,12 @@
         src = (wg_hbm, wv_hbm)[which]
         cols = pl.ds(pl.multiple_of((lane * chunks + c) * cw, LANES), cw)
         return pltpu.make_async_copy(
-            src.at[l, :, cols], w.at[l, c, lane, :, pl.ds(which * cw, cw)], wsem.at[l, c]
+            src.at[l, :, cols], w.at[l, c, lane, :, pl.ds(which * cw, cw)], wsem.at[jnp.where(l == 0, c, chunks + l - 1)]
         )
 
     def dcopy(l, lane, c):
         units = pl.ds(pl.multiple_of((lane * chunks + c) * cw, LANES), cw)
-        return pltpu.make_async_copy(dn_hbm.at[l, units, :], dn.at[l, c, lane], dsem.at[l, c])
+        return pltpu.make_async_copy(dn_hbm.at[l, units, :], dn.at[l, c, lane], dsem.at[l])
 
     def remote(src, dst, ss, rs, **to):
         return pltpu.make_async_remote_copy(
@@ -76,47 +91,47 @@
 
     def part_copy(l, h, lane, c):
         return remote(
-            part.at[h, lane, c], part.at[h, lane, c], p_ss.at[l, h, lane], rs_rs.at[h, lane, c], dp=MIX
+            part.at[h, lane, c], part.at[h, lane, c], p_ss.at[h, lane], rs_rs.at[h, lane, c], dp=MIX
         )
 
     def rs_copy(l, h, lane, c):
         return remote(
             rs_send.at[l, h, lane, c], rs_recv.at[l, h, lane, c],
-            rs_ss.at[l, h, lane], rs_rs.at[h, lane, c], ra=toward(lane, False), dp=MIX,
+            rs_ss.at[h, lane], rs_rs.at[h, lane, c], ra=toward(lane, False), dp=MIX,
         )
 
     def ag_copy(l, h, lane, c):
         return remote(
             hid.at[l, h, lane, c], hid.at[l, h, lane, c],
-            ag_ss.at[l, h, lane], ag_rs.at[h, lane, c], ra=toward(lane, True), dp=MIX,
+            ag_ss.at[h, lane], ag_rs.at[h, lane, c], ra=toward(lane, True), dp=MIX,
         )
 
     def sq_copy(l, h, e):
         return remote(
-            sq_send.at[l, h], sq_recv.at[l, h, me], sq_ss.at[l, h, e], sq_rs.at[l, h],
+            sq_send.at[l, h], sq_recv.at[l, h, me], sq_ss.at[h], sq_rs.at[h],
             ra=(0, n - 1)[e], dp=MIX,
         )
 
     def t_copy(l, h, o):
         to = lax.rem(mc + o, m)
-        return remote(tbuf.at[l, h, own(to)], rbuf.at[l, h, o], t_ss.at[l, h], t_rs.at[l, h], cb=to)
+        return remote(tbuf.at[l, h, own(to)], rbuf.at[l, h, o], t_ss.at[h], t_rs.at[h], cb=to)
 
     def n_copy(l, h, o):
         mine = own(mc)
         return remote(
-            snew.at[l, h, mine], snew.at[l, h, mine], n_ss.at[l, h], n_rs.at[l, h],
+            snew.at[l, h, mine], snew.at[l, h, mine], n_ss.at[h], n_rs.at[h],
             cb=lax.rem(mc + o, m), dp=UP,
         )
 
     def full_copy(h):
         return remote(
-            s_in.at[pl.ds((h - half) * rows, rows)], snew.at[0, h], i_ss.at[h], i_rs.at[h], dp=UP
+            s_in.at[pl.ds((h - half) * rows, rows)], snew.at[0, h], i_ss.at[0], i_rs.at[0], dp=UP
         )
 
     def mine_copy(h):
         return remote(
             s_in.at[pl.ds(pl.multiple_of(h * rows + mc * rq, rq), rq)], snew.at[0, h, own(mc)],
-            i_ss.at[h], i_rs.at[h], dp=MIX,
+            i_ss.at[0], i_rs.at[0], dp=MIX,
         )
 
     def fsq_copy(h, r, o):
@@ -154,40 +169,58 @@
     def greet(**to):
         pl.semaphore_signal(barrier, inc=1, device_id=to, device_id_type=MESH)
 
+    def fetch(x):
+        return pltpu.make_async_copy(ins[x], held[x], xsem.at[x])
+
+    near = 1 + jnp.where(me > 0, 1, 0) + jnp.where(me < n - 1, 1, 0)
+
     @pl.when(core == UP)
     def _():
         for o in range(m):
             greet(cb=lax.rem(mc + o, m), dp=MIX)
+        for x in (0, 1, 6):
+            fetch(x).start()
+        for lane in range(2):
+            for which in range(2):
+                wcopy(0, lane, 0, which).start()
 
     @pl.when(core == MIX)
     def _():
-        for o in range(n):
-            greet(ra=lax.rem(me + o, n), dp=UP)
+        greet(dp=UP)
+
+        @pl.when(me > 0)
+        def _():
+            greet(ra=me - 1, dp=UP)
+
+        @pl.when(me < n - 1)
+        def _():
+            greet(ra=me + 1, dp=UP)
+
         for o in range(1, n):
             greet(ra=lax.rem(me + o, n), dp=MIX)
         for o in range(1, m):
             greet(cb=lax.rem(mc + o, m), dp=MIX)
+        for x in (0, 2, 3, 4, 5, 6):
+            fetch(x).start()
 
     @pl.when(core == UP)
     def _():
-        for c in range(chunks):
+        for x in (0, 1, 6):
+            fetch(x).wait()
+        for c in range(1, chunks):
             for lane in range(2):
                 for which in range(2):
                     wcopy(0, lane, c, which).start()
+        for h in range(half):
+            snew[0, h] = s_in[h * rows : (h + 1) * rows]
 
     @pl.when(core == MIX)
     def _():
+        for x in (0, 2, 3, 4, 5, 6):
+            fetch(x).wait()
         for c in range(chunks):
             for lane in range(2):
                 dcopy(0, lane, c).start()
-
-    @pl.when(core == UP)
-    def _():
-        for h in range(half):
-            snew[0, h] = s_in[h * rows : (h + 1) * rows]
-
-    @pl.when(core == MIX)
-    def _():
         mine = own(mc)
         for h in range(half, groups):
             snew[0, h, mine] = s_in[pl.ds(pl.multiple_of((h - half) * rows + mc * rq, rq), rq)]
@@ -204,10 +237,6 @@
 
     @pl.when(core == UP)
     def _():
-        pl.semaphore_wait(barrier, n)
-        for h in range(half):
-            mine_copy(h).start()
-
         first = jnp.where(me == 0, 1, 0)
 
         def item(i, carry):
@@ -218,13 +247,9 @@
 
             @pl.when(c == 0)
             def _():
-                @pl.when((l == 0) & (h >= half))
-                def _():
-                    full_copy(h).wait_recv()
-
                 @pl.when(l > 0)
                 def _():
-                    arrived(snew.at[l, h], n_rs.at[l, h])
+                    arrived(snew.at[l, h], n_rs.at[h])
 
                 gain = ng[0:1, :].astype(f32)
                 for x in range(1, layers):
@@ -233,7 +258,14 @@
 
             @pl.when(h == 0)
             def _():
-                pltpu.make_async_copy(w.at[l, c], w.at[l, c], wsem.at[l, c]).wait()
+                @pl.when(l == 0)
+                def _():
+                    pltpu.make_async_copy(w.at[0, c], w.at[0, c], wsem.at[c]).wait()
+
+                @pl.when((l > 0) & (c == 0))
+                def _():
+                    pltpu.make_async_copy(w.at[l], w.at[l], wsem.at[chunks + l - 1]).wait()
+
 
             for a in range(2):
                 lane = first if a == 0 else 1 - first
@@ -246,20 +278,49 @@
 
                     @pl.when(k == 0)
                     def _():
+                        @pl.when((l > 0) & (c == 0))
+                        def _():
+                            left(rs_send.at[0, h, lane], rs_ss.at[h, lane])
+
                         rs_send[l, h, lane, c] = up().astype(bf16)
+
+                @pl.when(k > 0)
+                def _():
+                    @pl.when((l > 0) & (c == 0))
+                    def _():
+                        left(part.at[h, lane], p_ss.at[h, lane])
+
+                    part[h, lane, c] = up()
+
+                if a == 0:
+
+                    @pl.when(i == 0)
+                    def _():
+                        pl.semaphore_wait(barrier, near)
+
+                    @pl.when(k == 0)
+                    def _():
                         rs_copy(l, h, lane, c).start()
 
                 @pl.when(k > 0)
                 def _():
-                    @pl.when((l > 0) & (c == 0))
-                    def _():
-                        left(part.at[h, lane], p_ss.at[l - 1, h, lane])
-
-                    part[h, lane, c] = up()
                     part_copy(l, h, lane, c).start()
 
-            @pl.when(c == 0)
-            def _():
+            @pl.when(i == 0)
+            def _():
+                for x in range(half):
+                    mine_copy(x).start()
+
+            @pl.when(i == chunks - 2)
+            def _():
+                arrived(snew.at[0, half:groups], i_rs.at[0])
+
+            @pl.when(c == chunks - 2)
+            def _():
+                @pl.when(l > 0)
+                def _():
+                    left(sq_send.at[0:2, 0], sq_ss.at[h])
+
                 values = snew[l, h].astype(f32)
                 total = jnp.sum(values * values, axis=1, keepdims=True)
                 square = jnp.broadcast_to(jnp.concatenate([total] * (LANES // rows), axis=0), (LANES, LANES))
@@ -285,18 +346,14 @@
 
                 @pl.when(k == 0)
                 def _():
-                    for l in range(layers):
-                        left(rs_send.at[l, h, lane], rs_ss.at[l, h, lane])
+                    left(rs_send.at[0, h, lane], rs_ss.at[h, lane])
 
                 @pl.when(k > 0)
                 def _():
-                    left(part.at[h, lane], p_ss.at[layers - 1, h, lane])
-
-            for l in range(layers):
-                for e in range(2):
-                    sq_copy(l, h, e).wait_send()
-        for h in range(half):
-            mine_copy(h).wait_send()
+                    left(part.at[h, lane], p_ss.at[h, lane])
+
+            left(sq_send.at[0:2, 0], sq_ss.at[h])
+        left(raw.at[:, own(0)], i_ss.at[0])
         for h in range(half):
             arrived(raw.at[h], f_rs.at[h])
             arrived(fsq_recv.at[h], fs_rs.at[h])
@@ -304,7 +361,7 @@
 
     @pl.when(core == MIX)
     def _():
-        pl.semaphore_wait(barrier, n + 2 * m - 2)
+        pl.semaphore_wait(barrier, n - 1 + 2 * m - 1)
         for h in range(half, groups):
             full_copy(h).start()
 
@@ -318,31 +375,37 @@
             return result
 
         def finish_scale(l, h):
-            arrived(sq_recv.at[l, h], sq_rs.at[l, h])
+            arrived(sq_recv.at[l, h], sq_rs.at[h])
             total = jnp.zeros((8, LANES), f32)
             for r in range(n):
                 total = total + sq_recv[l, h, r]
             inverse = lax.rsqrt(total / width + EPS)
             scale[...] = jnp.broadcast_to(inverse[0:1], (LANES, LANES)).T[0:rows]
 
-        def split(i):
-            at = jnp.maximum(i, 0)
-            l = at // period
-            rest = at - l * period
-            valid = (i >= 0) & (l < layers) & (rest < items)
-            l = jnp.minimum(l, layers - 1)
-            rest = jnp.minimum(rest, items - 1)
+        def split(starts, i):
+            at = i * 0
+            for g, start in enumerate(starts):
+                inside = (i >= start) & (i < start + chunks)
+                valid = inside if g == 0 else valid | inside
+                at = jnp.where(inside, g * chunks + i - start, at)
+            l = at // items
+            rest = at - l * items
             h = rest // chunks
             return valid, l, h, rest - h * chunks
 
-        def later(i):
-            last = (layers - 1) * period
-            return jnp.where(i < last, i, jnp.where(i < last + LAST_BACK, -1, i - LAST_BACK))
+        def due(times, i):
+            valid = i == times[0]
+            at = i * 0
+            for g, time in enumerate(times):
+                valid = valid | (i == time)
+                at = jnp.where(i == time, g, at)
+            l = at // groups
+            return valid, l, at - l * groups
 
         def step(t, carry):
             for lane in range(2):
                 k = place(lane)
-                valid, l, h, c = split(t - SKEW * (k - 1))
+                valid, l, h, c = split(sums, t - SKEW * (k - 1))
 
                 @pl.when(valid & (k > 0))
                 def _():
@@ -370,7 +433,7 @@
 
             for lane in range(2):
                 k = place(lane)
-                valid, l, h, c = split(later(t - off_owner - SKEW_BACK * (n - 1 - k)))
+                valid, l, h, c = split(backs, t - SKEW_BACK * (n - 1 - k))
 
                 @pl.when(valid & (k < n - 1))
                 def _():
@@ -380,24 +443,17 @@
                     def _():
                         ag_copy(l, h, lane, c).start()
 
-            i = jnp.maximum(later(t - off_own), 0)
-            l = i // period
-            rest = i - l * period
-            tardy = jnp.where(l < layers - 1, OWN_EXTRA, 0)
-            fires = jnp.where(
-                rest < items - 1, lax.rem(rest, chunks) == chunks - 1, rest == items - 1 + tardy
-            )
-            h = jnp.minimum(rest // chunks, groups - 1)
-
-            @pl.when(fires & (l < layers))
+            valid, l, h = due(owns, t)
+
+            @pl.when(valid)
             def _():
                 mine = own(mc)
 
-                @pl.when((l == 0) & (h < half))
-                def _():
-                    mine_copy(h).wait_recv()
-
-                arrived(rbuf.at[l, h, 1:m], t_rs.at[l, h])
+                @pl.when((l == 0) & (h == 0))
+                def _():
+                    arrived(raw.at[:, own(0)], i_rs.at[0])
+
+                arrived(rbuf.at[l, h, 1:m], t_rs.at[h])
                 total = tbuf[l, h, mine].astype(f32)
                 for o in range(1, m):
                     total = total + rbuf[l, h, o].astype(f32)
@@ -405,6 +461,10 @@
 
                 @pl.when(l < layers - 1)
                 def _():
+                    @pl.when(l > 0)
+                    def _():
+                        left(snew.at[0, h], n_ss.at[h])
+
                     snew[l + 1, h, mine] = new
                     for o in range(m):
                         n_copy(l + 1, h, o).start()
@@ -412,40 +472,39 @@
                 @pl.when(l == layers - 1)
                 def _():
                     fin[h] = new
-                    for o in range(1, m):
-                        f_copy(h, o).start()
                     values = new.astype(f32)
                     square = jnp.sum(values * values, axis=1, keepdims=True)
                     square = jnp.broadcast_to(jnp.concatenate([square] * (LANES // rq), axis=0), (LANES, LANES))
                     fsq_send[h] = square.T[0:1]
 
-                    @pl.when(h < half)
-                    def _():
-                        f_copy(h, 0).start()
-                        fsq_copy(h, 0, 0).start()
-
-                    @pl.when(h >= half)
-                    def _():
-                        raw[h - half, mine] = new
-                        fsq_recv[h - half, me * m + mc] = fsq_send[h]
-
-                    for o in range(1, m):
-                        fsq_copy(h, 0, o).start()
-
                     def spread(r, carry):
                         for o in range(m):
                             fsq_copy(h, r, o).start()
                         return carry
 
                     lax.fori_loop(1, n, spread, 0)
-
-            valid, l, h, c = split(later(t - off_down))
+                    for o in range(1, m):
+                        fsq_copy(h, 0, o).start()
+                    for o in range(1, m):
+                        f_copy(h, o).start()
+
+                    @pl.when(h < half)
+                    def _():
+                        f_copy(h, 0).start()
+                        fsq_copy(h, 0, 0).start()
+
+                    @pl.when(h >= half)
+                    def _():
+                        raw[h - half, mine] = new
+                        fsq_recv[h - half, me * m + mc] = fsq_send[h]
+
+            valid, l, h, c = split(backs, t - SKEW_BACK * (n - 1))
 
             @pl.when(valid)
             def _():
-                @pl.when(h == 0)
-                def _():
-                    pltpu.make_async_copy(dn.at[l, c], dn.at[l, c], dsem.at[l, c]).wait()
+                @pl.when((h == 0) & (c == 0))
+                def _():
+                    pltpu.make_async_copy(dn.at[l], dn.at[l], dsem.at[l]).wait()
 
                 acc[...] += jnp.dot(hid[l, h, 0, c], dn[l, c, 0], preferred_element_type=f32) + jnp.dot(
                     hid[l, h, 1, c], dn[l, c, 1], preferred_element_type=f32
@@ -454,6 +513,11 @@
                 @pl.when(c == chunks - 1)
                 def _():
                     tbuf[l, h] = acc[...].astype(bf16)
+
+                    @pl.when(l > 0)
+                    def _():
+                        left(tbuf.at[0, h, 0 : rows - rq], t_ss.at[h])
+
                     for o in range(1, m):
                         t_copy(l, h, o).start()
                     acc[...] = jnp.zeros(acc.shape, f32)
@@ -462,22 +526,21 @@
 
                         @pl.when((k > 0) & (k < n - 1))
                         def _():
-                            left(rs_send.at[l, h, lane], rs_ss.at[l, h, lane])
+                            left(rs_send.at[l, h, lane], rs_ss.at[h, lane])
 
                         @pl.when(k > 0)
                         def _():
-                            left(hid.at[l, h, lane], ag_ss.at[l, h, lane])
-
-            valid, l, h, c = split(later(t - off_end))
-
-            @pl.when(valid & (c == chunks - 1) & (l == layers - 1) & (h >= half))
-            def _():
+                            left(hid.at[l, h, lane], ag_ss.at[h, lane])
+
+            @pl.when(t > max(owns))
+            def _():
+                h = half + t - max(owns) - 1
                 at = h - half
                 arrived(raw.at[at, 0 : rows - rq], f_rs.at[h])
                 arrived(fsq_recv.at[at, 1 : n * m], fs_rs.at[h])
                 end(h)
 
-            @pl.when(t == chunks - 1)
+            @pl.when(t == begin + chunks - 1)
             def _():
                 for x in range(1, layers):
                     for cc in range(chunks):
@@ -486,15 +549,13 @@
 
             return carry
 
-        lax.fori_loop(0, (layers - 1) * period + items + off_end + LAST_BACK, step, 0)
-
-        for h in range(half, groups):
-            full_copy(h).wait_send()
+        lax.fori_loop(begin, finish, step, 0)
+
+        left(raw, i_ss.at[0])
         for h in range(groups):
-            for l in range(layers):
-                left(tbuf.at[l, h, 0 : rows - rq], t_ss.at[l, h])
-                if l:
-                    left(snew.at[l, h], n_ss.at[l, h])
+            left(tbuf.at[0, h, 0 : rows - rq], t_ss.at[h])
+            if layers > 1:
+                left(snew.at[0, h], n_ss.at[h])
             home = h // half
             left(raw.at[0, 0 : rows - home * rq], f_ss.at[h])
             left(fsq_recv.at[0, home : n * m], fs_ss.at[h])
@@ -514,12 +575,16 @@
     hbm = pl.BlockSpec(memory_space=pl.ANY)
     dma = pltpu.SemaphoreType.DMA
     pieces = (layers, groups, 2, chunks)
+    small = (
+        stream.reshape(batch * length, dl), norm_gain, gate_taps.swapaxes(0, 1), value_taps.swapaxes(0, 1),
+        gate_bias, value_bias, final_gain,
+    )
     result = pl.pallas_call(
         functools.partial(chain_kernel, (n, m, width)),
         out_shape=jax.ShapeDtypeStruct((batch * length, dl), bf16),
-        in_specs=[vmem] * 7 + [hbm] * 3,
+        in_specs=[hbm] * 10,
         out_specs=vmem,
-        scratch_shapes=[
+        scratch_shapes=[pltpu.VMEM(x.shape, bf16) for x in small] + [
             pltpu.VMEM((layers, chunks, 2, dl, 2 * cw), bf16),
             pltpu.VMEM((layers, chunks, 2, cw, dl), bf16),
             pltpu.VMEM((rows, dl), bf16),
@@ -539,22 +604,16 @@
             pltpu.VMEM((groups // 2, rows, dl), bf16),
             pltpu.VMEM((groups, 1, LANES), f32),
             pltpu.VMEM((groups // 2, n * m, 1, LANES), f32),
-            dma((layers, chunks)),
-            dma((layers, chunks)),
-            dma(pieces[:3]), dma(pieces[:3]), dma(pieces[1:]), dma(pieces[:3]), dma(pieces[1:]),
-            dma((layers, groups, 2)), dma((layers, groups)),
-            dma((layers, groups)), dma((layers, groups)),
-            dma((layers, groups)), dma((layers, groups)),
-            dma((groups,)), dma((groups,)),
-            dma((groups,)), dma((groups,)),
-            dma((groups,)), dma((groups,)),
+            dma((chunks + layers - 1,)), dma((layers,)), dma((7,)),
+            dma((groups, 2)), dma((groups, 2)), dma(pieces[1:]), dma((groups, 2)), dma(pieces[1:]),
+            dma((groups,)), dma((groups,)), dma((groups,)), dma((groups,)), dma((groups,)), dma((groups,)),
+            dma((1,)), dma((1,)), dma((groups,)), dma((groups,)), dma((groups,)), dma((groups,)),
         ],
         compiler_params=pltpu.CompilerParams(
             collective_id=0, has_side_effects=True, vmem_limit_bytes=67_000_000
         ),
     )(
-        stream.reshape(batch * length, dl), norm_gain, gate_taps.swapaxes(0, 1), value_taps.swapaxes(0, 1),
-        gate_bias, value_bias, final_gain, gate_weight, value_weight, down_weight,
+        *small, gate_weight, value_weight, down_weight,
     )
     return result.reshape(batch, length, dl)
 

time: 87.6 us -> 83.8 us (0.957)
  Pallas kernels: 85.8 us -> 81.9 us
    pallas_call x1, Pallas kernels: 85.8 us -> 81.9 us  [body(): pl.pallas_call(functools.partial(chain_kernel, (n, m, width)), out_shape=...]
where the time goes in v3:
time: 83.8 us; the launch traced here: 83.6 us
  Pallas kernels  81.9 us (98%)
  local copies, waits for them, and re-layouts  1.67 us (2%)
    pallas_call x1, Pallas kernels, body(): pl.pallas_call(functools.partial(chain_kernel, (n, m, width)), out_shape=...  81.9 us

profile of v3, /device:TPU:1, one launch (start us, length us, event | category | flops | bytes accessed | tf_op | source)
XLA Modules:
  0.0 83.6 jit_solution(16447904647096377175)
XLA Ops:
  0.0 81.9 %shard_map.100 = bf16[128,1024]{1,0:T(8,128)(2,1)} custom-call(bf16[128,1024]{1,0:T(8,128)(2,1)} %bitcast.5, bf16[2,1024]{1,0:T(2,128)(2,1)} %refs_1_.1, bf16[3,2,3072]{2,1,0:T(2,128)(2,1)} %bitcast.6, bf16[3,2,3072]{2,1,0:T(2,128)(2,1)} %bitcast.7, bf16[2,3072]{1,0:T(2,128)(2,1)} %refs_4_.1, bf16[2,3072]{1,0:T(2,128)(2,1)} %refs_5_.1, ...), custom_call_target="tpu_custom_call" | custom-call | tf_op jit(solution)/shard_map/pallas_call | solution.py:582
  81.9 1.7 %copy.12 = bf16[2,64,1024]{2,1,0:T(8,128)(2,1)} copy(bf16[2,64,1024]{2,1,0:T(8,128)(2,1)} %bitcast.4) | data formatting | bytes 524288

commit v4 on v3

--- a/solution.py
+++ b/solution.py
@@ -17,8 +17,8 @@
 NEXT_LAG = 7
 TUNED_FOR = (4, 6)
 SUMS = [0, 6, 13, 20, 31, 37, 44, 50]
-BACKS = [6, 13, 19, 25, 37, 43, 51, 57]
-OWNS = [24, 30, 36, 42, 59, 68, 72, 73]
+BACKS = [6, 13, 19, 25, 36, 42, 49, 55]
+OWNS = [24, 30, 36, 42, 59, 66, 70, 71]
 UP, MIX = 0, 1
 
 

time: 83.8 us -> 83.7 us (level)
  no operation moved by 1% of the time
where the time goes in v4:
time: 83.7 us; the launch traced here: 83.5 us
  Pallas kernels  81.8 us (98%)
  local copies, waits for them, and re-layouts  1.67 us (2%)
    pallas_call x1, Pallas kernels, body(): pl.pallas_call(functools.partial(chain_kernel, (n, m, width)), out_shape=...  81.8 us

profile of v4, /device:TPU:1, one launch (start us, length us, event | category | flops | bytes accessed | tf_op | source)
XLA Modules:
  0.0 83.5 jit_solution(1682626591562440446)
XLA Ops:
  0.0 81.8 %shard_map.100 = bf16[128,1024]{1,0:T(8,128)(2,1)} custom-call(bf16[128,1024]{1,0:T(8,128)(2,1)} %bitcast.5, bf16[2,1024]{1,0:T(2,128)(2,1)} %refs_1_.1, bf16[3,2,3072]{2,1,0:T(2,128)(2,1)} %bitcast.6, bf16[3,2,3072]{2,1,0:T(2,128)(2,1)} %bitcast.7, bf16[2,3072]{1,0:T(2,128)(2,1)} %refs_4_.1, bf16[2,3072]{1,0:T(2,128)(2,1)} %refs_5_.1, ...), custom_call_target="tpu_custom_call" | custom-call | tf_op jit(solution)/shard_map/pallas_call | solution.py:582
  81.8 1.7 %copy.12 = bf16[2,64,1024]{2,1,0:T(8,128)(2,1)} copy(bf16[2,64,1024]{2,1,0:T(8,128)(2,1)} %bitcast.4) | data formatting | bytes 524288
